TPU v7x, 32 devices: a whole 2x2x4 slice. The times are simulated.
32 devices in a mesh: kv: 4 (over y, x), tp: 8 (over z, core).
Axes of the slice: x: 2, y: 2, z: 4, core: 2. Of those that a mesh axis runs over, the one named last changes fastest.
Arguments:
- residual: bfloat16 [128, 4096], P(None, ('kv', 'tp')), may hold values from -20 to 20
- mixer_gain: float32 [4096], P('kv'), may hold values from 0.1 to 1.9
- w_query: bfloat16 [4096, 4096], P('kv', 'tp'), may hold values from -0.09375 to 0.09375
- w_forget: bfloat16 [4096, 4096], P('kv', 'tp'), may hold values from -0.09375 to 0.09375
- w_input: bfloat16 [4096, 4096], P('kv', 'tp'), may hold values from -0.09375 to 0.09375
- w_outgate: bfloat16 [4096, 4096], P('kv', 'tp'), may hold values from -0.09375 to 0.09375
- lower_bound: float32 [4096], P('tp'), may hold values from 0.3 to 0.97
- state: float32 [128, 32, 128, 128], P('kv', 'tp'), may hold values from -6 to 6
- head_gain: float32 [128], replicated, may hold values from 0.1 to 1.9
- w_mix_out: bfloat16 [4096, 4096], P('tp', 'kv'), may hold values from -0.09375 to 0.09375
- ffn_gain: float32 [4096], P('kv'), may hold values from 0.1 to 1.9
- w_gate: bfloat16 [4096, 10752], P('kv', 'tp'), may hold values from -0.09375 to 0.09375
- w_up: bfloat16 [4096, 10752], P('kv', 'tp'), may hold values from -0.09375 to 0.09375
- w_down: bfloat16 [10752, 4096], P('tp', 'kv'), may hold values from -0.0625 to 0.0625
Outputs:
- layer_out: bfloat16 [128, 4096], P(None, ('kv', 'tp'))
- new_state: float32 [128, 32, 128, 128], P('kv', 'tp')
All inputs are finite; a program needn't handle non-finite values.
Results may differ from a plain program's by a relative error of at most 0.015.
Values may be sent and summed in bfloat16 or wider, within the bound.
No kernel may reach another device: no remote copies, remote signals or barrier semaphores. Data moves between devices by JAX's collectives and lax.ppermute only.
A program may use at most 64 MiB of HBM per device.

v0:
```python
import jax
import jax.numpy as jnp
from jax import lax
from jax.sharding import PartitionSpec as P

D = 4096
DK = 128
DV = 128
EPS = 1e-06


def project_row(weight, piece):
    return jnp.dot(piece, weight, preferred_element_type=jnp.float32)


def channel_mix(rows_in, ffn_gain, w_gate, w_up, w_down):
    rows_float = rows_in.astype(jnp.float32)
    squares = jnp.sum(rows_float * rows_float, axis=1)
    scaled = (rows_float * ffn_gain).astype(jnp.bfloat16)
    gate = jnp.dot(scaled, w_gate, preferred_element_type=jnp.float32)
    upper = jnp.dot(scaled, w_up, preferred_element_type=jnp.float32)
    whole_total = lax.psum(squares, "kv")
    gate, upper = (
        lax.psum(gate.astype(jnp.bfloat16), "kv").astype(jnp.float32),
        lax.psum(upper.astype(jnp.bfloat16), "kv").astype(jnp.float32),
    )
    inverse = lax.rsqrt(whole_total / D + EPS)[:, None]
    hidden = (jax.nn.silu(gate * inverse) * (upper * inverse)).astype(jnp.bfloat16)
    terms = jnp.dot(hidden, w_down, preferred_element_type=jnp.float32)
    summed = lax.psum_scatter(
        terms.astype(jnp.bfloat16), "tp", scatter_dimension=1, tiled=True
    ).astype(jnp.float32)
    width = summed.shape[1]
    own = lax.dynamic_slice_in_dim(rows_float, lax.axis_index("tp") * width, width, 1)
    return (own + summed).astype(jnp.bfloat16)


def body(
    residual,
    mixer_gain,
    w_query,
    w_forget,
    w_input,
    w_outgate,
    lower_bound,
    state,
    head_gain,
    w_mix_out,
    ffn_gain,
    w_gate,
    w_up,
    w_down,
):
    local_seqs, local_heads = (state.shape[0], state.shape[1])
    rows = lax.all_gather(residual, "tp", axis=1, tiled=True)
    rows_float = rows.astype(jnp.float32)
    squares = jnp.sum(rows_float * rows_float, axis=1)
    scaled = (rows_float * mixer_gain).astype(jnp.bfloat16)
    part_query = jnp.dot(scaled, w_query, preferred_element_type=jnp.float32)
    part_forget = jnp.dot(scaled, w_forget, preferred_element_type=jnp.float32)
    part_value = jnp.dot(scaled, w_input, preferred_element_type=jnp.float32)
    part_gate = jnp.dot(scaled, w_outgate, preferred_element_type=jnp.float32)
    whole_total = lax.psum(squares, "kv")
    total = lax.dynamic_slice_in_dim(whole_total, lax.axis_index("kv") * local_seqs, local_seqs)
    part_query, part_forget, part_value, part_gate = (
        lax.psum_scatter(part_query, "kv", scatter_dimension=0, tiled=True),
        lax.psum_scatter(part_forget, "kv", scatter_dimension=0, tiled=True),
        lax.psum_scatter(part_value, "kv", scatter_dimension=0, tiled=True),
        lax.psum_scatter(part_gate, "kv", scatter_dimension=0, tiled=True),
    )
    inverse = lax.rsqrt(total / D + EPS)[:, None]
    bound = lower_bound.reshape(local_heads, DK)
    forget_raw = (part_forget * inverse).reshape(local_seqs, local_heads, DK)
    forget = bound + (1.0 - bound) * jax.nn.sigmoid(forget_raw)
    keyvec = (1.0 - bound) * jax.nn.sigmoid(-forget_raw)
    query = jax.nn.silu((part_query * inverse).reshape(local_seqs, local_heads, DK))
    values = (part_value * inverse).reshape(local_seqs, local_heads, DV)
    updated = forget[..., None] * state + keyvec[..., None] * values[:, :, None, :]
    head_out = jnp.einsum("shc,shce->she", query, updated, precision=lax.Precision.HIGHEST)
    inv_head = lax.rsqrt(jnp.mean(head_out * head_out, axis=2, keepdims=True) + EPS)
    out_gate = jax.nn.silu((part_gate * inverse).reshape(local_seqs, local_heads, DV))
    normed = (
        (head_out * inv_head * head_gain * out_gate)
        .reshape(local_seqs, local_heads * DV)
        .astype(jnp.bfloat16)
    )
    terms = project_row(w_mix_out, lax.all_gather(normed, "kv", axis=0, tiled=True))
    mixed = lax.psum(terms, "tp")
    after_mix = (rows_float + mixed).astype(jnp.bfloat16)
    layer_out = channel_mix(after_mix, ffn_gain, w_gate, w_up, w_down)
    return (layer_out, updated)


def solution(mesh):
    in_specs = (
        P(None, ("kv", "tp")),
        P("kv"),
        P("kv", "tp"),
        P("kv", "tp"),
        P("kv", "tp"),
        P("kv", "tp"),
        P("tp"),
        P("kv", "tp", None, None),
        P(),
        P("tp", "kv"),
        P("kv"),
        P("kv", "tp"),
        P("kv", "tp"),
        P("tp", "kv"),
    )
    out_specs = (P(None, ("kv", "tp")), P("kv", "tp", None, None))
    return jax.shard_map(body, mesh=mesh, in_specs=in_specs, out_specs=out_specs, check_vma=False)
```

profile of v0, /device:TPU:0, one launch (start us, length us, event | category | flops | bytes accessed | tf_op | source)
XLA Modules:
  0.0 312.9 jit_solution(12020792351462122957)
XLA Ops:
  7.2 0.0 copy-start
  7.2 0.0 reduce-scatter.10.cloned.1.call-start
  7.2 15.1 %all_gather.6 = bf16[128,1024]{1,0:T(8,128)(2,1)S(1)} all-gather(bf16[128,128]{1,0:T(8,128)(2,1)} %param.14), channel_id=1, replica_groups=mesh['kv'=4,'tp'=8] {'tp'}, dimensions={1}, use_global_device_ids=true | all-gather | bytes 294912 | tf_op jit(solution)/shard_map/all_gather | solution.py:55
  22.4 2.3 fusion.10
  24.6 0.0 reduce-scatter.10.cloned.1.call-update
  24.7 0.0 reduce-scatter.12.cloned.1.call-start
  24.7 2.2 fusion.8
  27.0 0.0 reduce-scatter.12.cloned.1.call-update
  27.0 0.0 reduce-scatter.14.cloned.1.call-start
  27.0 2.3 fusion.6
  29.3 0.0 reduce-scatter.14.cloned.1.call-update
  29.3 0.0 reduce-scatter.8.cloned.1.call-start
  29.4 2.3 fusion.12
  31.6 0.0 reduce-scatter.8.cloned.1.call-update
  31.7 0.0 all-reduce.4.cloned.1.call-start
  31.7 0.1 fusion.1
  31.8 9.9 %psum.35 = f32[128]{0:T(128)S(1)} all-reduce(f32[128]{0:T(128)S(1)} %fusion.1), channel_id=1, replica_groups=mesh['kv'=4,'tp'=8] {'kv'}, use_global_device_ids=true, to_apply=%region_2.0 | all-reduce | flops 128 | bytes 1024 | tf_op jit(solution)/shard_map/psum | solution.py:63
  41.8 0.1 add_rsqrt_fusion.2
  41.8 0.7 broadcast_subtract_fusion
  42.5 6.5 %reduce-scatter.10.cloned.1.call-done = f32[32,512]{1,0:T(8,128)} async-done(((f32[128,512]{1,0:T(8,128)}), f32[32,512]{1,0:T(8,128)}) %reduce-scatter.10.cloned.1.call-update) | async-done | bytes 65552 | tf_op jit(solution)/shard_map/reduce_scatter | solution.py:67
  49.0 27.1 %reduce-scatter.12.cloned.1.call-done = f32[32,512]{1,0:T(8,128)} async-done(((f32[128,512]{1,0:T(8,128)}), f32[32,512]{1,0:T(8,128)}) %reduce-scatter.12.cloned.1.call-update) | async-done | bytes 65552 | tf_op jit(solution)/shard_map/reduce_scatter | solution.py:68
  76.1 27.2 %reduce-scatter.14.cloned.1.call-done = f32[32,512]{1,0:T(8,128)} async-done(((f32[128,512]{1,0:T(8,128)}), f32[32,512]{1,0:T(8,128)}) %reduce-scatter.14.cloned.1.call-update) | async-done | bytes 65552 | tf_op jit(solution)/shard_map/reduce_scatter | solution.py:69
  103.3 27.0 %reduce-scatter.8.cloned.1.call-done = f32[32,512]{1,0:T(8,128)} async-done(((f32[128,512]{1,0:T(8,128)}), f32[32,512]{1,0:T(8,128)}) %reduce-scatter.8.cloned.1.call-update) | async-done | bytes 65552 | tf_op jit(solution)/shard_map/reduce_scatter | solution.py:66
  130.3 1.0 add_divide_fusion.1
  131.6 8.2 %multiply_add_fusion = f32[32,4,128,128]{3,2,1,0:T(8,128)S(1)} fusion(f32[32,4,128,128]{3,2,1,0:T(8,128)} %param.21, f32[32,4,128]{2,1,0:T(4,128)S(1)} %mul.164, f32[32,4,128]{2,1,0:T(4,128)S(1)} %bitcast.35, f32[32,4,128]{2,1,0:T(4,128)S(1)} %bitcast.34), kind=kLoop, calls=%fused_computation | loop fusion | flops 6291456 | bytes 16973824 | tf_op jit(solution)/shard_map/add | solution.py:78
  139.8 0.0 copy-start.1
  139.9 3.4 %copy-done.1 = f32[32,4,128,128]{3,2,1,0:T(8,128)} copy-done((f32[32,4,128,128]{3,2,1,0:T(8,128)}, f32[32,4,128,128]{3,2,1,0:T(8,128)S(1)}, u32[]{:S(2)}) %copy-start.1) | copy-done | bytes 8388632
  143.2 7.2 %fusion.18 = f32[32,4,1,128]{3,2,1,0:T(1,128)S(1)} fusion(f32[32,4,128,1]{2,3,1,0:T(1,128)S(1)} %bitcast.33, f32[32,4,128,128]{3,2,1,0:T(8,128)S(1)} %multiply_add_fusion), kind=kOutput, calls=%fused_computation.39 | convolution fusion | flops 25165824 | bytes 8519680 | tf_op jit(solution)/shard_map/shc,shce->she/dot_general | solution.py:79
  150.5 0.1 multiply_reduce_fusion.1
  150.6 0.1 fusion.15
  150.8 8.5 %all_gather.7 = bf16[128,512]{1,0:T(8,128)(2,1)S(1)} all-gather(bf16[32,512]{1,0:T(8,128)(2,1)S(1)} %bitcast.38), channel_id=1, replica_groups=mesh['kv'=4,'tp'=8] {'kv'}, dimensions={0}, use_global_device_ids=true | all-gather | bytes 163840 | tf_op jit(solution)/shard_map/all_gather | solution.py:87
  159.2 1.1 fusion.19
  160.4 0.0 all-reduce.4.cloned.1.call-update
  160.4 0.0 all-reduce.6.cloned.1.call-start
  160.4 56.7 %all-reduce.4.cloned.1.call-done = f32[128,1024]{1,0:T(8,128)} async-done(((f32[128,1024]{1,0:T(8,128)}), f32[128,1024]{1,0:T(8,128)}) %all-reduce.4.cloned.1.call-update) | async-done | bytes 524304 | tf_op jit(solution)/shard_map/psum | solution.py:88
  217.1 1.2 multiply_reduce_fusion
  218.3 1.6 convolution_convert_fusion
  219.9 3.4 %convolution_convert_fusion.1 = bf16[128,1344]{0,1:T(8,128)(2,1)} fusion(bf16[1024,1344]{0,1:T(8,128)(2,1)} %param.25, f32[128,1024]{1,0:T(8,128)S(1)} %get-tuple-element.5, f32[1024]{0:T(1024)S(1)} %copy-done.3), kind=kOutput, calls=%fused_computation.2 | convolution fusion | flops 352755712 | bytes 3624960 | tf_op jit(solution)/shard_map/dot_general | solution.py:20
  223.3 0.0 all-reduce.6.cloned.1.call-update
  223.4 0.0 reduce-scatter.16.cloned.1.call-start
  223.4 10.2 %psum.38 = f32[128]{0:T(128)S(1)} all-reduce(f32[128]{0:T(128)S(1)} %get-tuple-element.4), channel_id=1, replica_groups=mesh['kv'=4,'tp'=8] {'kv'}, use_global_device_ids=true, to_apply=%region_10.11 | all-reduce | flops 128 | bytes 1024 | tf_op jit(solution)/shard_map/psum | solution.py:22
  233.6 36.4 %all-reduce.6.cloned.1.call-done = (bf16[128,1344]{0,1:T(8,128)(2,1)}, bf16[128,1344]{0,1:T(8,128)(2,1)}) async-done(((bf16[128,1344]{0,1:T(8,128)(2,1)}, bf16[128,1344]{0,1:T(8,128)(2,1)}), (bf16[128,1344]{0,1:T(8,128)(2,1)}, bf16[128,1344]{0,1:T(8,128)(2,1)})) %all-reduce.6.cloned.1.call-update) | async-done | bytes 688144 | tf_op jit(solution)/shard_map/psum | solution.py:25
  270.0 2.8 convolution_convert_fusion.2
  272.7 0.8 copy.18
  273.6 0.0 reduce-scatter.16.cloned.1.call-update
  273.6 31.0 %reduce-scatter.16.cloned.1.call-done = bf16[128,128]{1,0:T(8,128)(2,1)} async-done(((bf16[1024,128]{1,0:T(8,128)(2,1)}), bf16[128,128]{1,0:T(8,128)(2,1)}) %reduce-scatter.16.cloned.1.call-update) | async-done | bytes 32784
  304.5 0.9 copy.19
  305.4 0.6 add_convert_fusion
  (21 shorter events, 0.2 us)
Async XLA Ops:
  7.2 211.1 %copy-start = (bf16[1024,1344]{0,1:T(8,128)(2,1)S(1)}, bf16[1024,1344]{0,1:T(8,128)(2,1)}, u32[]{:S(2)}) copy-start(bf16[1024,1344]{0,1:T(8,128)(2,1)} %param.26) | copy-start | bytes 8257540
  7.2 124.4 %copy-start.4 = (f32[512]{0:T(512)S(1)}, f32[512]{0:T(512)}, u32[]{:S(2)}) copy-start(f32[512]{0:T(512)} %param.20) | copy-start | bytes 6148
  7.2 41.8 %reduce-scatter.10.cloned.1.call-start = ((), (), s32[]{:S(2)}) async-start(), calls=%async_computation.6 | async-start | bytes 327680 | tf_op jit(solution)/shard_map/reduce_scatter | solution.py:67
  24.7 51.5 %reduce-scatter.12.cloned.1.call-start = ((), (), s32[]{:S(2)}) async-start(), calls=%async_computation.7 | async-start | bytes 327680 | tf_op jit(solution)/shard_map/reduce_scatter | solution.py:68
  27.0 76.3 %reduce-scatter.14.cloned.1.call-start = ((), (), s32[]{:S(2)}) async-start(), calls=%async_computation.8 | async-start | bytes 327680 | tf_op jit(solution)/shard_map/reduce_scatter | solution.py:69
  29.3 101.0 %reduce-scatter.8.cloned.1.call-start = ((), (), s32[]{:S(2)}) async-start(), calls=%async_computation.5 | async-start | bytes 327680 | tf_op jit(solution)/shard_map/reduce_scatter | solution.py:66
  31.7 185.4 %all-reduce.4.cloned.1.call-start = ((), (), s32[]{:S(2)}) async-start(), calls=%async_computation.9 | async-start | bytes 1048576 | tf_op jit(solution)/shard_map/psum | solution.py:88
  139.8 3.4 %copy-start.1 = (f32[32,4,128,128]{3,2,1,0:T(8,128)}, f32[32,4,128,128]{3,2,1,0:T(8,128)S(1)}, u32[]{:S(2)}) copy-start(f32[32,4,128,128]{3,2,1,0:T(8,128)S(1)} %multiply_add_fusion) | copy-start | bytes 25165828
  139.8 10.8 %copy-start.5 = (f32[128]{0:T(128)S(1)}, f32[128]{0:T(128)}, u32[]{:S(2)}) copy-start(f32[128]{0:T(128)} %param.22) | copy-start | bytes 1540
  139.9 19.4 %copy-start.2 = (bf16[512,1024]{1,0:T(8,128)(2,1)S(1)}, bf16[512,1024]{1,0:T(8,128)(2,1)}, u32[]{:S(2)}) copy-start(bf16[512,1024]{1,0:T(8,128)(2,1)} %param.23) | copy-start | bytes 3145732
  139.9 78.4 %copy-start.3 = (f32[1024]{0:T(1024)S(1)}, f32[1024]{0:T(1024)}, u32[]{:S(2)}) copy-start(f32[1024]{0:T(1024)} %param.24) | copy-start | bytes 12292
  160.4 109.6 %all-reduce.6.cloned.1.call-start = ((), (), s32[]{:S(2)}) async-start(), calls=%async_computation.11 | async-start | bytes 1376256 | tf_op jit(solution)/shard_map/psum | solution.py:25
  223.4 81.2 %reduce-scatter.16.cloned.1.call-start = ((), (), s32[]{:S(2)}) async-start(), calls=%async_computation.10 | async-start | bytes 294912
Sparse Core Ops, SparseCore 0:
  24.8 24.1 reduce-scatter.9
  51.7 24.3 reduce-scatter.11
  78.9 24.3 reduce-scatter.13
  105.9 24.3 reduce-scatter.7
  160.5 56.5 all-reduce.3
  223.5 46.4 all-reduce.5
  273.7 30.7 reduce-scatter.15
where the time goes:
time: 314 us; the launch traced here: 313 us
  waiting for transfers between devices  212 us (68%)
  blocking collectives  43.7 us (14%)
  matrix products  25.2 us (8%)
  between operations  14.3 us (5%)
  other arithmetic  12.3 us (4%)
  local copies, waits for them, and re-layouts  5.22 us (2%)
    psum x1, waiting for transfers between devices, body(): mixed = lax.psum(terms, 'tp')  56.7 us
    psum x1, waiting for transfers between devices, channel_mix(): lax.psum(upper.astype(jnp.bfloat16), 'kv').astype(jnp.float32)  36.4 us
    unnamed x8, waiting for transfers between devices  31.1 us
    reduce_scatter x1, waiting for transfers between devices, body(): lax.psum_scatter(part_gate, 'kv', scatter_dimension=0, tiled=True)  27.2 us
    reduce_scatter x1, waiting for transfers between devices, body(): lax.psum_scatter(part_value, 'kv', scatter_dimension=0, tiled=True)  27.1 us
    reduce_scatter x1, waiting for transfers between devices, body(): lax.psum_scatter(part_query, 'kv', scatter_dimension=0, tiled=True)  27 us
    all_gather x1, blocking collectives, body(): rows = lax.all_gather(residual, 'tp', axis=1, tiled=True)  15.1 us
    psum x1, blocking collectives, channel_mix(): whole_total = lax.psum(squares, 'kv')  10.2 us
  transfers between devices with their start and end apart: 7, of which 7 were waited for; matrix products, arithmetic and copies ran while one was open for 2% of the time, Pallas kernels for 0%

commit v1 on v0

--- a/solution.py
+++ b/solution.py
@@ -2,6 +2,7 @@
 import jax.numpy as jnp
 from jax import lax
 from jax.sharding import PartitionSpec as P
+from jax.lax import all_gather
 
 D = 4096
 DK = 128
@@ -85,7 +86,7 @@
         .astype(jnp.bfloat16)
     )
     terms = project_row(w_mix_out, lax.all_gather(normed, "kv", axis=0, tiled=True))
-    mixed = lax.psum(terms, "tp")
+    mixed = jnp.sum(all_gather(terms, "tp"), axis=0)
     after_mix = (rows_float + mixed).astype(jnp.bfloat16)
     layer_out = channel_mix(after_mix, ffn_gain, w_gate, w_up, w_down)
     return (layer_out, updated)

time: 314 us -> 302 us (0.962)
  waiting for transfers between devices: 212 us -> 203 us
  local copies, waits for them, and re-layouts: 5.22 us -> 1.87 us
    psum x1 -> x0, waiting for transfers between devices: 56.7 us -> none  [body(): mixed = lax.psum(terms, 'tp')]
    all_gather x0 -> x1, waiting for transfers between devices: none -> 47 us  [body(): mixed = jnp.sum(all_gather(terms, 'tp'), axis=0)]
    reduce_sum x0 -> x1, other arithmetic: none -> 3.4 us  [body(): mixed = jnp.sum(all_gather(terms, 'tp'), axis=0)]
    unnamed x17 -> x21, local copies, waits for them, and re-layouts: 5.09 us -> 1.75 us
where the time goes in v1:
time: 302 us; the launch traced here: 301 us
  waiting for transfers between devices  203 us (67%)
  blocking collectives  43.7 us (14%)
  matrix products  23.4 us (8%)
  other arithmetic  15.2 us (5%)
  between operations  14.4 us (5%)
    all_gather x1, waiting for transfers between devices, body(): mixed = jnp.sum(all_gather(terms, 'tp'), axis=0)  47 us
    psum x1, waiting for transfers between devices, channel_mix(): lax.psum(upper.astype(jnp.bfloat16), 'kv').astype(jnp.float32)  36.1 us
    unnamed x8, waiting for transfers between devices  31.1 us
    reduce_scatter x1, waiting for transfers between devices, body(): lax.psum_scatter(part_gate, 'kv', scatter_dimension=0, tiled=True)  27.1 us
    reduce_scatter x1, waiting for transfers between devices, body(): lax.psum_scatter(part_value, 'kv', scatter_dimension=0, tiled=True)  27.1 us
    reduce_scatter x1, waiting for transfers between devices, body(): lax.psum_scatter(part_query, 'kv', scatter_dimension=0, tiled=True)  27 us
    all_gather x1, blocking collectives, body(): rows = lax.all_gather(residual, 'tp', axis=1, tiled=True)  15.1 us
    psum x1, blocking collectives, channel_mix(): whole_total = lax.psum(squares, 'kv')  10.2 us
  transfers between devices with their start and end apart: 7, of which 7 were waited for; matrix products, arithmetic and copies ran while one was open for 2% of the time, Pallas kernels for 0%

profile of v1, /device:TPU:0, one launch (start us, length us, event | category | flops | bytes accessed | tf_op | source)
XLA Modules:
  0.0 301.3 jit_solution(16050818123356955633)
XLA Ops:
  7.2 0.0 copy-start
  7.2 0.0 reduce-scatter.10.cloned.1.call-start
  7.2 15.1 %all_gather.12 = bf16[128,1024]{1,0:T(8,128)(2,1)S(1)} all-gather(bf16[128,128]{1,0:T(8,128)(2,1)} %param.14), channel_id=1, replica_groups=mesh['kv'=4,'tp'=8] {'tp'}, dimensions={1}, use_global_device_ids=true | all-gather | bytes 294912 | tf_op jit(solution)/shard_map/all_gather | solution.py:56
  22.4 2.3 fusion.10
  24.7 0.0 reduce-scatter.10.cloned.1.call-update
  24.7 0.0 reduce-scatter.12.cloned.1.call-start
  24.7 2.2 fusion.8
  27.0 0.0 reduce-scatter.12.cloned.1.call-update
  27.0 0.0 reduce-scatter.14.cloned.1.call-start
  27.1 2.3 fusion.6
  29.3 0.0 reduce-scatter.14.cloned.1.call-update
  29.3 0.0 reduce-scatter.8.cloned.1.call-start
  29.4 2.2 fusion.12
  31.6 0.0 reduce-scatter.8.cloned.1.call-update
  31.7 0.0 all-gather.3.cloned.1.call-start
  31.7 0.1 fusion.1
  31.8 9.9 %psum.28 = f32[128]{0:T(128)S(1)} all-reduce(f32[128]{0:T(128)S(1)} %fusion.1), channel_id=1, replica_groups=mesh['kv'=4,'tp'=8] {'kv'}, use_global_device_ids=true, to_apply=%region_2.0 | all-reduce | flops 128 | bytes 1024 | tf_op jit(solution)/shard_map/psum | solution.py:64
  41.8 0.1 add_rsqrt_fusion.2
  41.8 7.1 %reduce-scatter.10.cloned.1.call-done = f32[32,512]{1,0:T(8,128)} async-done(((f32[128,512]{1,0:T(8,128)}), f32[32,512]{1,0:T(8,128)}) %reduce-scatter.10.cloned.1.call-update) | async-done | bytes 65552 | tf_op jit(solution)/shard_map/reduce_scatter | solution.py:68
  49.0 27.1 %reduce-scatter.12.cloned.1.call-done = f32[32,512]{1,0:T(8,128)} async-done(((f32[128,512]{1,0:T(8,128)}), f32[32,512]{1,0:T(8,128)}) %reduce-scatter.12.cloned.1.call-update) | async-done | bytes 65552 | tf_op jit(solution)/shard_map/reduce_scatter | solution.py:69
  76.1 27.1 %reduce-scatter.14.cloned.1.call-done = f32[32,512]{1,0:T(8,128)} async-done(((f32[128,512]{1,0:T(8,128)}), f32[32,512]{1,0:T(8,128)}) %reduce-scatter.14.cloned.1.call-update) | async-done | bytes 65552 | tf_op jit(solution)/shard_map/reduce_scatter | solution.py:70
  103.2 27.0 %reduce-scatter.8.cloned.1.call-done = f32[32,512]{1,0:T(8,128)} async-done(((f32[128,512]{1,0:T(8,128)}), f32[32,512]{1,0:T(8,128)}) %reduce-scatter.8.cloned.1.call-update) | async-done | bytes 65552 | tf_op jit(solution)/shard_map/reduce_scatter | solution.py:67
  130.2 1.0 add_divide_fusion.1
  131.5 8.2 %multiply_add_fusion = f32[32,4,128,128]{3,2,1,0:T(8,128)S(1)} fusion(f32[32,4,128,128]{3,2,1,0:T(8,128)} %param.21, f32[32,4,128]{2,1,0:T(4,128)S(1)} %mul.164, f32[32,4,128]{2,1,0:T(4,128)S(1)} %bitcast.37, f32[32,4,128]{2,1,0:T(4,128)S(1)} %bitcast.36), kind=kLoop, calls=%fused_computation | loop fusion | flops 6291456 | bytes 16973824 | tf_op jit(solution)/shard_map/add | solution.py:79
  139.7 0.0 copy-start.1
  139.8 0.0 copy-start.7
  139.8 7.2 %fusion.18 = f32[32,4,1,128]{3,2,1,0:T(1,128)S(1)} fusion(f32[32,4,128,1]{2,3,1,0:T(1,128)S(1)} %bitcast.35, f32[32,4,128,128]{3,2,1,0:T(8,128)S(1)} %multiply_add_fusion), kind=kOutput, calls=%fused_computation.39 | convolution fusion | flops 25165824 | bytes 8519680 | tf_op jit(solution)/shard_map/shc,shce->she/dot_general | solution.py:80
  147.0 0.1 multiply_reduce_fusion.1
  147.2 0.1 fusion.15
  147.3 8.5 %all_gather.13 = bf16[128,512]{1,0:T(8,128)(2,1)S(1)} all-gather(bf16[32,512]{1,0:T(8,128)(2,1)S(1)} %bitcast.40), channel_id=1, replica_groups=mesh['kv'=4,'tp'=8] {'kv'}, dimensions={0}, use_global_device_ids=true | all-gather | bytes 163840 | tf_op jit(solution)/shard_map/all_gather | solution.py:88
  155.8 1.1 fusion.19
  156.9 0.0 all-gather.3.cloned.1.call-update
  157.0 0.0 all-reduce.3.cloned.1.call-start
  157.0 47.0 %all-gather.3.cloned.1.call-done = f32[1024,1024]{1,0:T(8,128)} async-done(((f32[128,1024]{1,0:T(8,128)}), f32[1024,1024]{1,0:T(8,128)}) %all-gather.3.cloned.1.call-update) | async-done | bytes 4194320 | tf_op jit(solution)/shard_map/all_gather | solution.py:89
  204.0 3.4 %reduce_sum.38 = f32[128,1024]{1,0:T(8,128)} reduce(f32[8,128,1024]{2,1,0:T(8,128)} %bitcast.31, f32[]{:T(128)} %constant.11.clone.1), dimensions={0}, to_apply=%region_7.8 | reduce | flops 917504 | bytes 4718596 | tf_op jit(solution)/shard_map/reduce_sum | solution.py:89
  207.4 1.3 multiply_reduce_fusion
  208.7 1.6 convolution_convert_fusion
  210.4 1.6 convolution_convert_fusion.1
  212.0 0.0 all-reduce.3.cloned.1.call-update
  212.0 0.0 reduce-scatter.16.cloned.1.call-start
  212.1 10.2 %psum.30 = f32[128]{0:T(128)S(1)} all-reduce(f32[128]{0:T(128)S(1)} %get-tuple-element.4), channel_id=1, replica_groups=mesh['kv'=4,'tp'=8] {'kv'}, use_global_device_ids=true, to_apply=%region_10.11 | all-reduce | flops 128 | bytes 1024 | tf_op jit(solution)/shard_map/psum | solution.py:23
  222.2 36.1 %all-reduce.3.cloned.1.call-done = (bf16[128,1344]{0,1:T(8,128)(2,1)}, bf16[128,1344]{0,1:T(8,128)(2,1)}) async-done(((bf16[128,1344]{0,1:T(8,128)(2,1)}, bf16[128,1344]{0,1:T(8,128)(2,1)}), (bf16[128,1344]{0,1:T(8,128)(2,1)}, bf16[128,1344]{0,1:T(8,128)(2,1)})) %all-reduce.3.cloned.1.call-update) | async-done | bytes 688144 | tf_op jit(solution)/shard_map/psum | solution.py:26
  258.4 2.8 convolution_convert_fusion.2
  261.1 0.8 copy.18
  262.0 0.0 reduce-scatter.16.cloned.1.call-update
  262.0 31.0 %reduce-scatter.16.cloned.1.call-done = bf16[128,128]{1,0:T(8,128)(2,1)} async-done(((bf16[1024,128]{1,0:T(8,128)(2,1)}), bf16[128,128]{1,0:T(8,128)(2,1)}) %reduce-scatter.16.cloned.1.call-update) | async-done | bytes 32784
  293.0 0.9 copy.19
  293.9 0.6 add_convert_fusion
  (26 shorter events, 0.2 us)
Async XLA Ops:
  7.2 201.6 %copy-start = (bf16[1024,1344]{0,1:T(8,128)(2,1)S(1)}, bf16[1024,1344]{0,1:T(8,128)(2,1)}, u32[]{:S(2)}) copy-start(bf16[1024,1344]{0,1:T(8,128)(2,1)} %param.26) | copy-start | bytes 8257540
  7.2 22.2 %copy-start.4 = (f32[1024]{0:T(1024)S(1)}, f32[1024]{0:T(1024)}, u32[]{:S(2)}) copy-start(f32[1024]{0:T(1024)} %param.15) | copy-start | bytes 12292
  7.2 34.7 %copy-start.6 = (f32[512]{0:T(512)S(1)}, f32[512]{0:T(512)}, u32[]{:S(2)}) copy-start(f32[512]{0:T(512)} %param.20) | copy-start | bytes 6148
  7.2 41.8 %reduce-scatter.10.cloned.1.call-start = ((), (), s32[]{:S(2)}) async-start(), calls=%async_computation.6 | async-start | bytes 327680 | tf_op jit(solution)/shard_map/reduce_scatter | solution.py:68
  24.7 51.4 %reduce-scatter.12.cloned.1.call-start = ((), (), s32[]{:S(2)}) async-start(), calls=%async_computation.7 | async-start | bytes 327680 | tf_op jit(solution)/shard_map/reduce_scatter | solution.py:69
  27.0 76.2 %reduce-scatter.14.cloned.1.call-start = ((), (), s32[]{:S(2)}) async-start(), calls=%async_computation.8 | async-start | bytes 327680 | tf_op jit(solution)/shard_map/reduce_scatter | solution.py:70
  29.3 100.9 %reduce-scatter.8.cloned.1.call-start = ((), (), s32[]{:S(2)}) async-start(), calls=%async_computation.5 | async-start | bytes 327680 | tf_op jit(solution)/shard_map/reduce_scatter | solution.py:67
  31.7 172.3 %all-gather.3.cloned.1.call-start = ((), (), s32[]{:S(2)}) async-start(), calls=%async_computation.9 | async-start | bytes 4718592 | tf_op jit(solution)/shard_map/all_gather | solution.py:89
  139.7 7.3 %copy-start.1 = (f32[32,4,128,128]{3,2,1,0:T(8,128)}, f32[32,4,128,128]{3,2,1,0:T(8,128)S(1)}, u32[]{:S(2)}) copy-start(f32[32,4,128,128]{3,2,1,0:T(8,128)S(1)} %multiply_add_fusion) | copy-start | bytes 25165828
  139.8 7.4 %copy-start.7 = (f32[128]{0:T(128)S(1)}, f32[128]{0:T(128)}, u32[]{:S(2)}) copy-start(f32[128]{0:T(128)} %param.22) | copy-start | bytes 1540
  139.8 16.1 %copy-start.3 = (bf16[512,1024]{1,0:T(8,128)(2,1)S(1)}, bf16[512,1024]{1,0:T(8,128)(2,1)}, u32[]{:S(2)}) copy-start(bf16[512,1024]{1,0:T(8,128)(2,1)} %param.23) | copy-start | bytes 3145732
  147.3 61.4 %copy-start.5 = (f32[1024]{0:T(1024)S(1)}, f32[1024]{0:T(1024)}, u32[]{:S(2)}) copy-start(f32[1024]{0:T(1024)} %param.24) | copy-start | bytes 12292
  157.0 101.4 %all-reduce.3.cloned.1.call-start = ((), (), s32[]{:S(2)}) async-start(), calls=%async_computation.11 | async-start | bytes 1376256 | tf_op jit(solution)/shard_map/psum | solution.py:26
  207.4 3.0 copy-start.2
  212.0 81.0 %reduce-scatter.16.cloned.1.call-start = ((), (), s32[]{:S(2)}) async-start(), calls=%async_computation.10 | async-start | bytes 294912
Sparse Core Ops, SparseCore 0:
  24.8 24.1 reduce-scatter.9
  51.8 24.3 reduce-scatter.11
  78.9 24.3 reduce-scatter.13
  105.8 24.3 reduce-scatter.7
  157.1 46.8 all-gather.2
  212.1 46.2 all-reduce.2
  262.1 30.8 reduce-scatter.15
